TPU v7x, 32 devices: a whole 2x2x4 slice. The times are simulated.
32 devices in a mesh: kv: 4 (over y, x), tp: 8 (over z, core).
Axes of the slice: x: 2, y: 2, z: 4, core: 2. Of those that a mesh axis runs over, the one named last changes fastest.
Arguments:
- tokens: bfloat16 [256, 4096], P(None, ('kv', 'tp')), may hold values from -10 to 10
- past_state: float32 [256, 32, 64, 128], P('kv', 'tp'), may hold values from -6 to 6
- first_gain: float32 [4096], P('kv'), may hold values from 0.1 to 1.9
- first_gate: bfloat16 [4096, 11264], P('kv', 'tp'), may hold values from -0.09375 to 0.09375
- first_up: bfloat16 [4096, 11264], P('kv', 'tp'), may hold values from -0.09375 to 0.09375
- first_down: bfloat16 [11264, 4096], P('tp', 'kv'), may hold values from -0.078125 to 0.078125
- mix_gain: float32 [4096], P('kv'), may hold values from 0.1 to 1.9
- query_weight: bfloat16 [4096, 2048], P('kv', 'tp'), may hold values from -0.09375 to 0.09375
- key_weight: bfloat16 [4096, 2048], P('kv', 'tp'), may hold values from -0.09375 to 0.09375
- value_weight: bfloat16 [4096, 4096], P('kv', 'tp'), may hold values from -0.09375 to 0.09375
- output_gate_weight: bfloat16 [4096, 4096], P('kv', 'tp'), may hold values from -0.09375 to 0.09375
- head_gain: float32 [4096], P('tp'), may hold values from 0.1 to 1.9
- out_weight: bfloat16 [4096, 4096], P('tp', 'kv'), may hold values from -0.125 to 0.125
- second_gain: float32 [4096], P('kv'), may hold values from 0.1 to 1.9
- second_gate: bfloat16 [4096, 11264], P('kv', 'tp'), may hold values from -0.09375 to 0.09375
- second_up: bfloat16 [4096, 11264], P('kv', 'tp'), may hold values from -0.09375 to 0.09375
- second_down: bfloat16 [11264, 4096], P('tp', 'kv'), may hold values from -0.078125 to 0.078125
Outputs:
- mixed: bfloat16 [256, 4096], P(None, ('kv', 'tp'))
- new_state: float32 [256, 32, 64, 128], P('kv', 'tp')
All inputs are finite; a program needn't handle non-finite values.
Results may differ from a plain program's by a relative error of at most 0.033.
Values may be sent and summed in bfloat16 or wider, within the bound.
A program may use at most 128 MiB of HBM per device.

v0:
```python
import jax
import jax.numpy as jnp
from jax import lax
from jax.sharding import PartitionSpec as P

D = 4096
HEADS = 32
HEAD_K = 64
HEAD_V = 128
POS = 16384
EPS_RMS = 1e-06
EPS_GROUP = 1e-05
ROPE_BASE = 10000.0


def rotate(vectors):
    half_width = vectors.shape[-1] // 2
    frequency = ROPE_BASE ** (-jnp.arange(half_width, dtype=jnp.float32) / half_width)
    angles = POS * frequency
    cosine = jnp.cos(angles)
    sine_part = jnp.sin(angles)
    lower = vectors[..., :half_width]
    upper = vectors[..., half_width:]
    return jnp.concatenate(
        [lower * cosine - upper * sine_part, lower * sine_part + upper * cosine], axis=-1
    )


def activate(gate_sum, up_sum, summed):
    inverse_rms = lax.rsqrt(summed / D + EPS_RMS)[:, None]
    return (jax.nn.silu(gate_sum * inverse_rms) * (up_sum * inverse_rms)).astype(jnp.bfloat16)


def channel_mix(widened, gain, w_gate, w_up, w_down):
    widened_f = widened.astype(jnp.float32)
    scaled = (widened_f * gain).astype(jnp.bfloat16)
    squares = jnp.sum(widened_f * widened_f, axis=1)
    gate_part = jnp.dot(scaled, w_gate, preferred_element_type=jnp.float32)
    up_part = jnp.dot(scaled, w_up, preferred_element_type=jnp.float32)
    gate_sum, up_sum, summed = (
        lax.psum(gate_part.astype(jnp.bfloat16), "kv").astype(jnp.float32),
        lax.psum(up_part.astype(jnp.bfloat16), "kv").astype(jnp.float32),
        lax.psum(squares.astype(jnp.bfloat16), "kv").astype(jnp.float32),
    )
    return 0.5 * jnp.dot(
        activate(gate_sum, up_sum, summed), w_down, preferred_element_type=jnp.float32
    )


def token_mix(
    widened,
    past_state,
    gain,
    query_weight,
    key_weight,
    value_weight,
    output_gate_weight,
    head_gain,
    out_weight,
):
    widened_f = widened.astype(jnp.float32)
    scaled = (widened_f * gain).astype(jnp.bfloat16)
    squares = jnp.sum(widened_f * widened_f, axis=1)
    query_part = jnp.dot(scaled, query_weight, preferred_element_type=jnp.float32)
    key_part = jnp.dot(scaled, key_weight, preferred_element_type=jnp.float32)
    value_part = jnp.dot(scaled, value_weight, preferred_element_type=jnp.float32)
    gate_part = jnp.dot(scaled, output_gate_weight, preferred_element_type=jnp.float32)
    queries, keys_now, values_now, gate_now, summed = (
        lax.psum_scatter(
            query_part.astype(jnp.bfloat16), "kv", scatter_dimension=0, tiled=True
        ).astype(jnp.float32),
        lax.psum_scatter(
            key_part.astype(jnp.bfloat16), "kv", scatter_dimension=0, tiled=True
        ).astype(jnp.float32),
        lax.psum_scatter(
            value_part.astype(jnp.bfloat16), "kv", scatter_dimension=0, tiled=True
        ).astype(jnp.float32),
        lax.psum_scatter(
            gate_part.astype(jnp.bfloat16), "kv", scatter_dimension=0, tiled=True
        ).astype(jnp.float32),
        lax.psum_scatter(
            squares.astype(jnp.bfloat16), "kv", scatter_dimension=0, tiled=True
        ).astype(jnp.float32),
    )
    inverse_rms = lax.rsqrt(summed / D + EPS_RMS)[:, None]
    row_count = past_state.shape[0]
    local_heads = past_state.shape[1]
    queries = rotate((queries * inverse_rms).reshape(row_count, local_heads, HEAD_K)) * HEAD_K ** (
        -0.5
    )
    keys_now = rotate((keys_now * inverse_rms).reshape(row_count, local_heads, HEAD_K))
    values_now = (values_now * inverse_rms).reshape(row_count, local_heads, HEAD_V)
    gate_now = gate_now * inverse_rms
    head_level = (lax.axis_index("tp") * local_heads + jnp.arange(local_heads)).astype(jnp.float32)
    retained = 1.0 - jnp.exp2(-5.0 - 16.0 * head_level / (HEADS - 1))
    new_state = (
        retained[None, :, None, None] * past_state
        + keys_now[:, :, :, None] * values_now[:, :, None, :]
    )
    retrieved = jnp.einsum("bhk,bhkv->bhv", queries, new_state, precision=lax.Precision.HIGHEST)
    head_mean = jnp.mean(retrieved, axis=-1, keepdims=True)
    variance = jnp.mean(jnp.square(retrieved - head_mean), axis=-1, keepdims=True)
    normed = ((retrieved - head_mean) * lax.rsqrt(variance + EPS_GROUP)).reshape(
        row_count, local_heads * HEAD_V
    )
    mixed_heads = (jax.nn.silu(gate_now) * (normed * head_gain)).astype(jnp.bfloat16)
    projected = jnp.dot(
        lax.all_gather(mixed_heads, "kv", axis=0, tiled=True),
        out_weight,
        preferred_element_type=jnp.float32,
    )
    return (projected, new_state)


def shards(
    tokens,
    past_state,
    first_gain,
    first_gate,
    first_up,
    first_down,
    mix_gain,
    query_weight,
    key_weight,
    value_weight,
    output_gate_weight,
    head_gain,
    out_weight,
    second_gain,
    second_gate,
    second_up,
    second_down,
):

    def first_section(widened):
        return (channel_mix(widened, first_gain, first_gate, first_up, first_down), None)

    def middle_section(widened):
        return token_mix(
            widened,
            past_state,
            mix_gain,
            query_weight,
            key_weight,
            value_weight,
            output_gate_weight,
            head_gain,
            out_weight,
        )

    def last_section(widened):
        return (channel_mix(widened, second_gain, second_gate, second_up, second_down), None)

    sections = [first_section, middle_section, last_section]
    own_columns = tokens
    widened = lax.all_gather(tokens, "tp", axis=1, tiled=True)
    state_out = past_state
    for section_index in range(3):
        branch_out, produced = sections[section_index](widened)
        if produced is not None:
            state_out = produced
        own_piece = lax.psum_scatter(
            branch_out.astype(jnp.bfloat16), "tp", scatter_dimension=1, tiled=True
        ).astype(jnp.float32)
        own_columns = (own_columns.astype(jnp.float32) + own_piece).astype(jnp.bfloat16)
        if section_index < 2:
            widened = lax.all_gather(own_columns, "tp", axis=1, tiled=True)
    return (own_columns, state_out)


def solution(mesh):
    in_specs = (
        P(None, ("kv", "tp")),
        P("kv", "tp", None, None),
        P("kv"),
        P("kv", "tp"),
        P("kv", "tp"),
        P("tp", "kv"),
        P("kv"),
        P("kv", "tp"),
        P("kv", "tp"),
        P("kv", "tp"),
        P("kv", "tp"),
        P("tp"),
        P("tp", "kv"),
        P("kv"),
        P("kv", "tp"),
        P("kv", "tp"),
        P("tp", "kv"),
    )
    out_specs = (P(None, ("kv", "tp")), P("kv", "tp", None, None))
    return jax.shard_map(shards, mesh=mesh, in_specs=in_specs, out_specs=out_specs, check_vma=False)
```

profile of v0, /device:TPU:0, one launch (start us, length us, event | category | flops | bytes accessed | tf_op | source)
XLA Modules:
  0.0 409.7 jit_solution(10858656113238108868)
XLA Ops:
  7.2 15.8 %all_gather.12 = bf16[256,1024]{1,0:T(8,128)(2,1)S(1)} all-gather(bf16[256,128]{1,0:T(8,128)(2,1)} %param.17), channel_id=1, replica_groups=mesh['kv'=4,'tp'=8] {'tp'}, dimensions={1}, use_global_device_ids=true | all-gather | bytes 589824 | tf_op jit(solution)/shard_map/all_gather | solution.py:156
  23.0 2.5 convolution_convert_fusion.2
  25.6 1.9 convolution_convert_fusion.3
  27.7 10.1 %psum.43 = bf16[256]{0:T(256)(128)(2,1)S(1)} all-reduce(bf16[256]{0:T(256)(128)(2,1)S(1)} %fusion.3), channel_id=1, replica_groups=mesh['kv'=4,'tp'=8] {'kv'}, use_global_device_ids=true, to_apply=%region_2.0 | all-reduce | flops 256 | bytes 1024 | tf_op jit(solution)/shard_map/psum | solution.py:43
  37.8 48.4 %all-reduce.8.cloned.1.call-done = (bf16[256,1408]{1,0:T(8,128)(2,1)}, bf16[256,1408]{1,0:T(8,128)(2,1)}) async-done(((bf16[256,1408]{1,0:T(8,128)(2,1)}, bf16[256,1408]{1,0:T(8,128)(2,1)}), (bf16[256,1408]{1,0:T(8,128)(2,1)}, bf16[256,1408]{1,0:T(8,128)(2,1)})) %all-reduce.8.cloned.1.call-update) | async-done | bytes 1441808 | tf_op jit(solution)/shard_map/psum | solution.py:42
  86.2 3.5 fusion
  89.7 1.0 copy.24
  90.8 31.2 %reduce-scatter.22.cloned.1.call-done = bf16[128,256]{1,0:T(8,128)(2,1)} async-done(((bf16[1024,256]{1,0:T(8,128)(2,1)}), bf16[128,256]{1,0:T(8,128)(2,1)}) %reduce-scatter.22.cloned.1.call-update) | async-done | bytes 65552
  123.0 14.0 %all_gather.13 = bf16[256,1024]{1,0:T(8,128)(2,1)S(1)} all-gather(bf16[256,128]{1,0:T(8,128)(2,1)S(1)} %add_convert_fusion.2), channel_id=1, replica_groups=mesh['kv'=4,'tp'=8] {'tp'}, dimensions={1}, use_global_device_ids=true | all-gather | bytes 589824 | tf_op jit(solution)/shard_map/all_gather | solution.py:167
  137.1 2.0 convolution_convert_fusion.8
  140.4 2.0 convolution_convert_fusion.7
  142.5 2.4 convolution_convert_fusion.5
  145.1 9.9 %all-reduce = bf16[256]{0:T(256)(128)(2,1)S(1)} all-reduce(bf16[256]{0:T(256)(128)(2,1)S(1)} %fusion.5), channel_id=4, replica_groups=mesh['kv'=4,'tp'=8] {'kv'}, use_global_device_ids=true, to_apply=%region_7.8.clone | all-reduce | flops 256 | bytes 1024
  155.2 2.4 convolution_convert_fusion.6
  157.8 4.2 %reduce-scatter.16.cloned.1.call-done = bf16[64,256]{1,0:T(8,128)(2,1)} async-done(((bf16[256,256]{1,0:T(8,128)(2,1)}), bf16[64,256]{1,0:T(8,128)(2,1)}) %reduce-scatter.16.cloned.1.call-update) | async-done | bytes 32784 | tf_op jit(solution)/shard_map/reduce_scatter | solution.py:69
  162.0 26.8 %reduce-scatter.18.cloned.1.call-done = bf16[64,256]{1,0:T(8,128)(2,1)} async-done(((bf16[256,256]{1,0:T(8,128)(2,1)}), bf16[64,256]{1,0:T(8,128)(2,1)}) %reduce-scatter.18.cloned.1.call-update) | async-done | bytes 32784 | tf_op jit(solution)/shard_map/reduce_scatter | solution.py:72
  190.2 26.1 %reduce-scatter.20.cloned.1.call-done = bf16[64,512]{1,0:T(8,128)(2,1)} async-done(((bf16[256,512]{1,0:T(8,128)(2,1)}), bf16[64,512]{1,0:T(8,128)(2,1)}) %reduce-scatter.20.cloned.1.call-update) | async-done | bytes 65552 | tf_op jit(solution)/shard_map/reduce_scatter | solution.py:75
  217.3 5.3 %multiply_add_fusion = f32[64,4,64,128]{3,2,1,0:T(8,128)S(1)} fusion(f32[64,4,64,128]{3,2,1,0:T(8,128)} %param.18, f32[64,4,128]{2,1,0:T(4,128)S(1)} %mul.290, f32[64,4,64]{2,1,0:T(4,128)S(1)} %copy.21, f32[4]{0:T(128)S(1)} %exponential_subtract_fusion), kind=kLoop, calls=%fused_computation | loop fusion | flops 6291456 | bytes 16973840 | tf_op jit(solution)/shard_map/add | solution.py:97
  222.6 7.3 %fusion.30 = f32[64,4,1,128]{3,2,1,0:T(1,128)S(1)} fusion(f32[64,4,64,1]{2,3,1,0:T(1,128)S(1)} %copy.22, f32[64,4,64,128]{3,2,1,0:T(8,128)S(1)} %multiply_add_fusion), kind=kOutput, calls=%fused_computation.64 | convolution fusion | flops 25165824 | bytes 8585216 | tf_op jit(solution)/shard_map/bhk,bhkv->bhv/dot_general | solution.py:100
  230.6 12.7 %reduce-scatter.14.cloned.1.call-done = bf16[64,512]{1,0:T(8,128)(2,1)} async-done(((bf16[256,512]{1,0:T(8,128)(2,1)}), bf16[64,512]{1,0:T(8,128)(2,1)}) %reduce-scatter.14.cloned.1.call-update) | async-done | bytes 65552 | tf_op jit(solution)/shard_map/reduce_scatter | solution.py:78
  244.3 9.3 %all_gather.14 = bf16[256,512]{1,0:T(8,128)(2,1)S(1)} all-gather(bf16[64,512]{1,0:T(8,128)(2,1)S(1)} %fusion.21), channel_id=1, replica_groups=mesh['kv'=4,'tp'=8] {'kv'}, dimensions={0}, use_global_device_ids=true | all-gather | bytes 327680 | tf_op jit(solution)/shard_map/all_gather | solution.py:108
  253.6 1.7 convolution_convert_fusion.4
  255.2 1.0 copy.26
  256.3 31.4 %reduce-scatter.24.cloned.1.call-done = bf16[128,256]{1,0:T(8,128)(2,1)} async-done(((bf16[1024,256]{1,0:T(8,128)(2,1)}), bf16[128,256]{1,0:T(8,128)(2,1)}) %reduce-scatter.24.cloned.1.call-update) | async-done | bytes 65552
  288.7 14.2 %all_gather.15 = bf16[256,1024]{1,0:T(8,128)(2,1)S(1)} all-gather(bf16[256,128]{1,0:T(8,128)(2,1)S(1)} %add_convert_fusion.1), channel_id=1, replica_groups=mesh['kv'=4,'tp'=8] {'tp'}, dimensions={1}, use_global_device_ids=true | all-gather | bytes 589824 | tf_op jit(solution)/shard_map/all_gather | solution.py:167
  302.8 3.7 convolution_convert_fusion
  306.5 1.9 convolution_convert_fusion.1
  308.6 10.2 %psum.46 = bf16[256]{0:T(256)(128)(2,1)S(1)} all-reduce(bf16[256]{0:T(256)(128)(2,1)S(1)} %fusion.7), channel_id=1, replica_groups=mesh['kv'=4,'tp'=8] {'kv'}, use_global_device_ids=true, to_apply=%region_16.17 | all-reduce | flops 256 | bytes 1024 | tf_op jit(solution)/shard_map/psum | solution.py:43
  318.9 46.7 %all-reduce.6.cloned.1.call-done = (bf16[256,1408]{1,0:T(8,128)(2,1)}, bf16[256,1408]{1,0:T(8,128)(2,1)}) async-done(((bf16[256,1408]{1,0:T(8,128)(2,1)}, bf16[256,1408]{1,0:T(8,128)(2,1)}), (bf16[256,1408]{1,0:T(8,128)(2,1)}, bf16[256,1408]{1,0:T(8,128)(2,1)})) %all-reduce.6.cloned.1.call-update) | async-done | bytes 1441808 | tf_op jit(solution)/shard_map/psum | solution.py:42
  365.6 3.4 fusion.1
  369.0 1.0 copy.28
  370.0 31.6 %reduce-scatter.26.cloned.1.call-done = bf16[128,256]{1,0:T(8,128)(2,1)} async-done(((bf16[1024,256]{1,0:T(8,128)(2,1)}), bf16[128,256]{1,0:T(8,128)(2,1)}) %reduce-scatter.26.cloned.1.call-update) | async-done | bytes 65552
  (69 shorter events, 9.5 us)
Async XLA Ops:
  7.2 15.9 %copy-start = (bf16[1024,1408]{1,0:T(8,128)(2,1)S(1)}, bf16[1024,1408]{1,0:T(8,128)(2,1)}, u32[]{:S(2)}) copy-start(bf16[1024,1408]{1,0:T(8,128)(2,1)} %param.21) | copy-start | bytes 8650756
  7.2 18.4 %copy-start.6 = (f32[1024]{0:T(1024)S(1)}, f32[1024]{0:T(1024)}, u32[]{:S(2)}) copy-start(f32[1024]{0:T(1024)} %param.19) | copy-start | bytes 12292
  7.2 79.0 %all-reduce.8.cloned.1.call-start = ((), (), s32[]{:S(2)}) async-start(), calls=%async_computation.15 | async-start | bytes 2883584 | tf_op jit(solution)/shard_map/psum | solution.py:42
  7.2 18.3 %copy-start.4 = (bf16[1024,1408]{1,0:T(8,128)(2,1)S(1)}, bf16[1024,1408]{1,0:T(8,128)(2,1)}, u32[]{:S(2)}) copy-start(bf16[1024,1408]{1,0:T(8,128)(2,1)} %param.20) | copy-start | bytes 8650756
  27.5 94.6 %reduce-scatter.22.cloned.1.call-start = ((), (), s32[]{:S(2)}) async-start(), calls=%async_computation.11 | async-start | bytes 589824
  86.2 36.8 %copy-start.2 = (bf16[256,128]{1,0:T(8,128)(2,1)S(1)}, bf16[256,128]{1,0:T(8,128)(2,1)}, u32[]{:S(2)}) copy-start(bf16[256,128]{1,0:T(8,128)(2,1)} %param.17) | copy-start | bytes 196612
  86.2 50.9 %copy-start.7 = (f32[1024]{0:T(1024)S(1)}, f32[1024]{0:T(1024)}, u32[]{:S(2)}) copy-start(f32[1024]{0:T(1024)} %param.23) | copy-start | bytes 12292
  89.7 49.5 %copy-start.9 = (u32[32]{0:T(128)S(1)}, u32[32]{0:T(128)}, u32[]{:S(2)}) copy-start(u32[32]{0:T(128)} %constant.53) | copy-start | bytes 388
  90.7 71.3 %reduce-scatter.16.cloned.1.call-start = ((), (), s32[]{:S(2)}) async-start(), calls=%async_computation.8 | async-start | bytes 163840 | tf_op jit(solution)/shard_map/reduce_scatter | solution.py:69
  139.1 49.7 %reduce-scatter.18.cloned.1.call-start = ((), (), s32[]{:S(2)}) async-start(), calls=%async_computation.9 | async-start | bytes 163840 | tf_op jit(solution)/shard_map/reduce_scatter | solution.py:72
  142.4 73.9 %reduce-scatter.20.cloned.1.call-start = ((), (), s32[]{:S(2)}) async-start(), calls=%async_computation.10 | async-start | bytes 327680 | tf_op jit(solution)/shard_map/reduce_scatter | solution.py:75
  144.9 98.4 %reduce-scatter.14.cloned.1.call-start = ((), (), s32[]{:S(2)}) async-start(), calls=%async_computation.7 | async-start | bytes 327680 | tf_op jit(solution)/shard_map/reduce_scatter | solution.py:78
  157.6 130.1 %reduce-scatter.24.cloned.1.call-start = ((), (), s32[]{:S(2)}) async-start(), calls=%async_computation.12 | async-start | bytes 589824
  222.6 7.4 %copy-start.1 = (f32[64,4,64,128]{3,2,1,0:T(8,128)}, f32[64,4,64,128]{3,2,1,0:T(8,128)S(1)}, u32[]{:S(2)}) copy-start(f32[64,4,64,128]{3,2,1,0:T(8,128)S(1)} %multiply_add_fusion) | copy-start | bytes 25165828
  222.6 20.7 %copy-start.3 = (f32[512]{0:T(512)S(1)}, f32[512]{0:T(512)}, u32[]{:S(2)}) copy-start(f32[512]{0:T(512)} %param.28) | copy-start | bytes 6148
  230.0 72.8 %copy-start.8 = (f32[1024]{0:T(1024)S(1)}, f32[1024]{0:T(1024)}, u32[]{:S(2)}) copy-start(f32[1024]{0:T(1024)} %param.30) | copy-start | bytes 12292
  256.2 109.3 %all-reduce.6.cloned.1.call-start = ((), (), s32[]{:S(2)}) async-start(), calls=%async_computation.14 | async-start | bytes 2883584 | tf_op jit(solution)/shard_map/psum | solution.py:42
  288.6 17.9 %copy-start.5 = (bf16[1024,1408]{1,0:T(8,128)(2,1)S(1)}, bf16[1024,1408]{1,0:T(8,128)(2,1)}, u32[]{:S(2)}) copy-start(bf16[1024,1408]{1,0:T(8,128)(2,1)} %param.31) | copy-start | bytes 8650756
  308.4 93.2 %reduce-scatter.26.cloned.1.call-start = ((), (), s32[]{:S(2)}) async-start(), calls=%async_computation.13 | async-start | bytes 589824
Sparse Core Ops, SparseCore 0:
  27.6 58.5 all-reduce.7
  90.8 31.1 reduce-scatter.21
  139.2 22.7 reduce-scatter.15
  164.6 24.1 reduce-scatter.17
  192.0 24.3 reduce-scatter.19
  218.9 24.3 reduce-scatter.13
  256.4 31.2 reduce-scatter.23
  308.5 56.9 all-reduce.5
  370.1 31.3 reduce-scatter.25
where the time goes:
time: 411 us; the launch traced here: 410 us
  waiting for transfers between devices  259 us (63%)
  blocking collectives  83.5 us (20%)
  matrix products  34.6 us (8%)
  between operations  14.8 us (4%)
  other arithmetic  10.2 us (2%)
  local copies, waits for them, and re-layouts  6.92 us (2%)
    psum x2, waiting for transfers between devices, channel_mix(): lax.psum(up_part.astype(jnp.bfloat16), 'kv').astype(jnp.float32)  95.1 us
    unnamed x12, waiting for transfers between devices  94.3 us
    all_gather x2, blocking collectives, shards(): widened = lax.all_gather(own_columns, 'tp', axis=1, tiled=True)  28.2 us
    reduce_scatter x1, waiting for transfers between devices, token_mix(): lax.psum_scatter(key_part.astype(jnp.bfloat16), 'kv', scatter_dimension=0...  26.8 us
    reduce_scatter x1, waiting for transfers between devices, token_mix(): lax.psum_scatter(value_part.astype(jnp.bfloat16), 'kv', scatter_dimension...  26.1 us
    psum x2, blocking collectives, channel_mix(): lax.psum(squares.astype(jnp.bfloat16), 'kv').astype(jnp.float32)  20.3 us
    all_gather x1, blocking collectives, shards(): widened = lax.all_gather(tokens, 'tp', axis=1, tiled=True)  15.8 us
    reduce_scatter x1, waiting for transfers between devices, token_mix(): lax.psum_scatter(gate_part.astype(jnp.bfloat16), 'kv', scatter_dimension=...  12.7 us
  transfers between devices with their start and end apart: 9, of which 9 were waited for; matrix products, arithmetic and copies ran while one was open for 6% of the time, Pallas kernels for 0%

commit v1 on v0

--- a/solution.py
+++ b/solution.py
@@ -164,7 +164,9 @@
         ).astype(jnp.float32)
         own_columns = (own_columns.astype(jnp.float32) + own_piece).astype(jnp.bfloat16)
         if section_index < 2:
-            widened = lax.all_gather(own_columns, "tp", axis=1, tiled=True)
+            widened = jnp.concatenate(
+                lax.all_to_all(jnp.stack([own_columns] * lax.axis_size("tp")), "tp", 0, 0), axis=1
+            )
     return (own_columns, state_out)
 
 

time: 411 us -> 422 us (1.027)
  waiting for transfers between devices: 259 us -> 275 us
  blocking collectives: 83.5 us -> 72.8 us
    all_gather x2 -> x0, blocking collectives: 28.2 us -> none  [shards(): widened = lax.all_gather(own_columns, 'tp', axis=1, tiled=True)]
    reduce_scatter x1, waiting for transfers between devices: 26.8 us -> 4.01 us  [token_mix(): lax.psum_scatter(key_part.astype(jnp.bfloat16), 'kv', scatter_dimension=0...]
    reduce_scatter x1, waiting for transfers between devices: 4.2 us -> 26.8 us  [token_mix(): lax.psum_scatter(query_part.astype(jnp.bfloat16), 'kv', scatter_dimension...]
    all_to_all x0 -> x1, blocking collectives: none -> 17.7 us  [shards(): lax.all_to_all(jnp.stack([own_columns] * lax.axis_size('tp')), 'tp', 0, 0)]
    all_to_all x0 -> x1, waiting for transfers between devices: none -> 15.1 us  [shards(): lax.all_to_all(jnp.stack([own_columns] * lax.axis_size('tp')), 'tp', 0, 0)]
  transfers between devices with their start and end apart: 9 -> 10, of which waited for: 9 -> 10; matrix products, arithmetic and copies ran while one was open for 6% -> 6% of each run, Pallas kernels for 0% -> 0%
where the time goes in v1:
time: 422 us; the launch traced here: 421 us
  waiting for transfers between devices  275 us (65%)
  blocking collectives  72.8 us (17%)
  matrix products  35.4 us (8%)
  between operations  14.8 us (4%)
  other arithmetic  10.5 us (2%)
  local copies, waits for them, and re-layouts  8.79 us (2%)
    psum x2, waiting for transfers between devices, channel_mix(): lax.psum(up_part.astype(jnp.bfloat16), 'kv').astype(jnp.float32)  95.6 us
    unnamed x12, waiting for transfers between devices  94.7 us
    reduce_scatter x1, waiting for transfers between devices, token_mix(): lax.psum_scatter(query_part.astype(jnp.bfloat16), 'kv', scatter_dimension...  26.8 us
    reduce_scatter x1, waiting for transfers between devices, token_mix(): lax.psum_scatter(value_part.astype(jnp.bfloat16), 'kv', scatter_dimension...  25.6 us
    psum x2, blocking collectives, channel_mix(): lax.psum(squares.astype(jnp.bfloat16), 'kv').astype(jnp.float32)  20.2 us
    all_to_all x1, blocking collectives, shards(): lax.all_to_all(jnp.stack([own_columns] * lax.axis_size('tp')), 'tp', 0, 0)  17.7 us
    all_gather x1, blocking collectives, shards(): widened = lax.all_gather(tokens, 'tp', axis=1, tiled=True)  15.8 us
    all_to_all x1, waiting for transfers between devices, shards(): lax.all_to_all(jnp.stack([own_columns] * lax.axis_size('tp')), 'tp', 0, 0)  15.1 us
  transfers between devices with their start and end apart: 10, of which 10 were waited for; matrix products, arithmetic and copies ran while one was open for 6% of the time, Pallas kernels for 0%

profile of v1, /device:TPU:0, one launch (start us, length us, event | category | flops | bytes accessed | tf_op | source)
XLA Modules:
  0.0 420.9 jit_solution(5804425401381459526)
XLA Ops:
  7.2 15.8 %all_gather.6 = bf16[256,1024]{1,0:T(8,128)(2,1)S(1)} all-gather(bf16[256,128]{1,0:T(8,128)(2,1)} %param.17), channel_id=1, replica_groups=mesh['kv'=4,'tp'=8] {'tp'}, dimensions={1}, use_global_device_ids=true | all-gather | bytes 589824 | tf_op jit(solution)/shard_map/all_gather | solution.py:156
  23.0 2.5 convolution_convert_fusion.2
  25.6 1.9 convolution_convert_fusion.3
  27.7 10.1 %psum.43 = bf16[256]{0:T(256)(128)(2,1)S(1)} all-reduce(bf16[256]{0:T(256)(128)(2,1)S(1)} %fusion.3), channel_id=1, replica_groups=mesh['kv'=4,'tp'=8] {'kv'}, use_global_device_ids=true, to_apply=%region_2.0 | all-reduce | flops 256 | bytes 1024 | tf_op jit(solution)/shard_map/psum | solution.py:43
  37.8 48.4 %all-reduce.8.cloned.1.call-done = (bf16[256,1408]{1,0:T(8,128)(2,1)}, bf16[256,1408]{1,0:T(8,128)(2,1)}) async-done(((bf16[256,1408]{1,0:T(8,128)(2,1)}, bf16[256,1408]{1,0:T(8,128)(2,1)}), (bf16[256,1408]{1,0:T(8,128)(2,1)}, bf16[256,1408]{1,0:T(8,128)(2,1)})) %all-reduce.8.cloned.1.call-update) | async-done | bytes 1441808 | tf_op jit(solution)/shard_map/psum | solution.py:42
  86.2 3.5 fusion
  89.7 1.0 copy.30
  90.7 31.6 %reduce-scatter.22.cloned.1.call-done = bf16[128,256]{1,0:T(8,128)(2,1)} async-done(((bf16[1024,256]{1,0:T(8,128)(2,1)}), bf16[128,256]{1,0:T(8,128)(2,1)}) %reduce-scatter.22.cloned.1.call-update) | async-done | bytes 65552
  124.2 3.5 all-to-all-start
  127.8 15.1 %all-to-all-done = bf16[8,256,128]{1,2,0:T(8,128)(2,1)S(1)} async-done(((bf16[8,256,128]{1,2,0:T(8,128)(2,1)}), bf16[8,256,128]{1,2,0:T(8,128)(2,1)S(1)}, u32[]{:S(2)}, u32[]{:S(2)}) %all-to-all-start) | async-done | bytes 524320 | tf_op jit(solution)/shard_map/all_to_all | solution.py:168
  144.0 2.0 convolution_convert_fusion.7
  147.4 2.2 convolution_convert_fusion.8
  149.6 2.5 convolution_convert_fusion.5
  152.4 9.8 %all-reduce = bf16[256]{0:T(256)(128)(2,1)S(1)} all-reduce(bf16[256]{0:T(256)(128)(2,1)S(1)} %multiply_reduce_fusion.1), channel_id=4, replica_groups=mesh['kv'=4,'tp'=8] {'kv'}, use_global_device_ids=true, to_apply=%region_7.8.clone | all-reduce | flops 256 | bytes 1024
  162.3 2.6 convolution_convert_fusion.6
  165.1 4.0 reduce-scatter.18.cloned.1.call-done
  169.1 26.8 %reduce-scatter.16.cloned.1.call-done = bf16[64,256]{1,0:T(8,128)(2,1)} async-done(((bf16[256,256]{1,0:T(8,128)(2,1)}), bf16[64,256]{1,0:T(8,128)(2,1)}) %reduce-scatter.16.cloned.1.call-update) | async-done | bytes 32784 | tf_op jit(solution)/shard_map/reduce_scatter | solution.py:69
  197.3 25.6 %reduce-scatter.20.cloned.1.call-done = bf16[64,512]{1,0:T(8,128)(2,1)} async-done(((bf16[256,512]{1,0:T(8,128)(2,1)}), bf16[64,512]{1,0:T(8,128)(2,1)}) %reduce-scatter.20.cloned.1.call-update) | async-done | bytes 65552 | tf_op jit(solution)/shard_map/reduce_scatter | solution.py:75
  223.8 5.3 %multiply_add_fusion = f32[64,4,64,128]{3,2,1,0:T(8,128)S(1)} fusion(f32[64,4,64,128]{3,2,1,0:T(8,128)} %param.18, f32[64,4,128]{2,1,0:T(4,128)S(1)} %mul.294, f32[64,4,64]{2,1,0:T(4,128)S(1)} %copy.26, f32[4]{0:T(128)S(1)} %exponential_subtract_fusion), kind=kLoop, calls=%fused_computation | loop fusion | flops 6291456 | bytes 16973840 | tf_op jit(solution)/shard_map/add | solution.py:97
  229.2 7.3 %fusion.22 = f32[64,4,1,128]{3,2,1,0:T(1,128)S(1)} fusion(f32[64,4,64,1]{2,3,1,0:T(1,128)S(1)} %copy.28, f32[64,4,64,128]{3,2,1,0:T(8,128)S(1)} %multiply_add_fusion), kind=kOutput, calls=%fused_computation.62 | convolution fusion | flops 25165824 | bytes 8585216 | tf_op jit(solution)/shard_map/bhk,bhkv->bhv/dot_general | solution.py:100
  237.1 12.7 %reduce-scatter.14.cloned.1.call-done = bf16[64,512]{1,0:T(8,128)(2,1)} async-done(((bf16[256,512]{1,0:T(8,128)(2,1)}), bf16[64,512]{1,0:T(8,128)(2,1)}) %reduce-scatter.14.cloned.1.call-update) | async-done | bytes 65552 | tf_op jit(solution)/shard_map/reduce_scatter | solution.py:78
  250.8 9.3 %all_gather.7 = bf16[256,512]{1,0:T(8,128)(2,1)S(1)} all-gather(bf16[64,512]{1,0:T(8,128)(2,1)S(1)} %fusion.13), channel_id=1, replica_groups=mesh['kv'=4,'tp'=8] {'kv'}, dimensions={0}, use_global_device_ids=true | all-gather | bytes 327680 | tf_op jit(solution)/shard_map/all_gather | solution.py:108
  260.1 1.7 convolution_convert_fusion.4
  261.7 1.0 copy.32
  262.8 31.4 %reduce-scatter.24.cloned.1.call-done = bf16[128,256]{1,0:T(8,128)(2,1)} async-done(((bf16[1024,256]{1,0:T(8,128)(2,1)}), bf16[128,256]{1,0:T(8,128)(2,1)}) %reduce-scatter.24.cloned.1.call-update) | async-done | bytes 65552
  295.4 17.7 %all_to_all.10 = bf16[8,256,128]{1,2,0:T(8,128)(2,1)S(1)} all-to-all(bf16[8,256,128]{1,2,0:T(8,128)(2,1)S(1)} %stack.5), channel_id=1, replica_groups=mesh['kv'=4,'tp'=8] {'tp'}, dimensions={0} | all-to-all | bytes 1048576 | tf_op jit(solution)/shard_map/all_to_all | solution.py:168
  313.3 3.9 convolution_convert_fusion
  317.2 1.9 convolution_convert_fusion.1
  319.3 10.1 %psum.46 = bf16[256]{0:T(256)(128)(2,1)S(1)} all-reduce(bf16[256]{0:T(256)(128)(2,1)S(1)} %multiply_reduce_fusion), channel_id=1, replica_groups=mesh['kv'=4,'tp'=8] {'kv'}, use_global_device_ids=true, to_apply=%region_16.17 | all-reduce | flops 256 | bytes 1024 | tf_op jit(solution)/shard_map/psum | solution.py:43
  329.5 47.2 %all-reduce.6.cloned.1.call-done = (bf16[256,1408]{1,0:T(8,128)(2,1)}, bf16[256,1408]{1,0:T(8,128)(2,1)}) async-done(((bf16[256,1408]{1,0:T(8,128)(2,1)}, bf16[256,1408]{1,0:T(8,128)(2,1)}), (bf16[256,1408]{1,0:T(8,128)(2,1)}, bf16[256,1408]{1,0:T(8,128)(2,1)})) %all-reduce.6.cloned.1.call-update) | async-done | bytes 1441808 | tf_op jit(solution)/shard_map/psum | solution.py:42
  376.7 3.4 fusion.1
  381.2 31.6 %reduce-scatter.26.cloned.1.call-done = bf16[128,256]{1,0:T(8,128)(2,1)} async-done(((bf16[1024,256]{1,0:T(8,128)(2,1)}), bf16[128,256]{1,0:T(8,128)(2,1)}) %reduce-scatter.26.cloned.1.call-update) | async-done | bytes 65552
  (78 shorter events, 12.7 us)
Async XLA Ops:
  7.2 15.9 %copy-start = (bf16[1024,1408]{1,0:T(8,128)(2,1)S(1)}, bf16[1024,1408]{1,0:T(8,128)(2,1)}, u32[]{:S(2)}) copy-start(bf16[1024,1408]{1,0:T(8,128)(2,1)} %param.21) | copy-start | bytes 8650756
  7.2 18.4 %copy-start.9 = (f32[1024]{0:T(1024)S(1)}, f32[1024]{0:T(1024)}, u32[]{:S(2)}) copy-start(f32[1024]{0:T(1024)} %param.19) | copy-start | bytes 12292
  7.2 79.0 %all-reduce.8.cloned.1.call-start = ((), (), s32[]{:S(2)}) async-start(), calls=%async_computation.17 | async-start | bytes 2883584 | tf_op jit(solution)/shard_map/psum | solution.py:42
  7.2 18.3 %copy-start.7 = (bf16[1024,1408]{1,0:T(8,128)(2,1)S(1)}, bf16[1024,1408]{1,0:T(8,128)(2,1)}, u32[]{:S(2)}) copy-start(bf16[1024,1408]{1,0:T(8,128)(2,1)} %param.20) | copy-start | bytes 8650756
  27.5 94.8 %reduce-scatter.22.cloned.1.call-start = ((), (), s32[]{:S(2)}) async-start(), calls=%async_computation.13 | async-start | bytes 589824
  86.2 37.0 %copy-start.3 = (bf16[256,128]{1,0:T(8,128)(2,1)S(1)}, bf16[256,128]{1,0:T(8,128)(2,1)}, u32[]{:S(2)}) copy-start(bf16[256,128]{1,0:T(8,128)(2,1)} %param.17) | copy-start | bytes 196612
  89.7 53.3 %copy-start.4 = (f32[1024]{0:T(1024)S(1)}, f32[1024]{0:T(1024)}, u32[]{:S(2)}) copy-start(f32[1024]{0:T(1024)} %param.23) | copy-start | bytes 12292
  89.7 56.4 %copy-start.10 = (u32[32]{0:T(128)S(1)}, u32[32]{0:T(128)}, u32[]{:S(2)}) copy-start(u32[32]{0:T(128)} %constant.53) | copy-start | bytes 388
  124.2 18.8 %all-to-all-start = ((bf16[8,256,128]{1,2,0:T(8,128)(2,1)}), bf16[8,256,128]{1,2,0:T(8,128)(2,1)S(1)}, u32[]{:S(2)}, u32[]{:S(2)}) async-start(bf16[8,256,128]{1,2,0:T(8,128)(2,1)} %stack.4), calls=%async_computation | async-start | bytes 1048576 | tf_op jit(solution)/shard_map/all_to_all | solution.py:168
  127.7 41.4 %reduce-scatter.18.cloned.1.call-start = ((), (), s32[]{:S(2)}) async-start(), calls=%async_computation.11 | async-start | bytes 163840 | tf_op jit(solution)/shard_map/reduce_scatter | solution.py:72
  143.2 0.8 copy-start.2
  146.0 49.8 %reduce-scatter.16.cloned.1.call-start = ((), (), s32[]{:S(2)}) async-start(), calls=%async_computation.10 | async-start | bytes 163840 | tf_op jit(solution)/shard_map/reduce_scatter | solution.py:69
  149.6 73.3 %reduce-scatter.20.cloned.1.call-start = ((), (), s32[]{:S(2)}) async-start(), calls=%async_computation.12 | async-start | bytes 327680 | tf_op jit(solution)/shard_map/reduce_scatter | solution.py:75
  152.2 97.7 %reduce-scatter.14.cloned.1.call-start = ((), (), s32[]{:S(2)}) async-start(), calls=%async_computation.9 | async-start | bytes 327680 | tf_op jit(solution)/shard_map/reduce_scatter | solution.py:78
  164.8 129.4 %reduce-scatter.24.cloned.1.call-start = ((), (), s32[]{:S(2)}) async-start(), calls=%async_computation.14 | async-start | bytes 589824
  229.2 7.4 %copy-start.1 = (f32[64,4,64,128]{3,2,1,0:T(8,128)}, f32[64,4,64,128]{3,2,1,0:T(8,128)S(1)}, u32[]{:S(2)}) copy-start(f32[64,4,64,128]{3,2,1,0:T(8,128)S(1)} %multiply_add_fusion) | copy-start | bytes 25165828
  229.2 20.7 %copy-start.6 = (f32[512]{0:T(512)S(1)}, f32[512]{0:T(512)}, u32[]{:S(2)}) copy-start(f32[512]{0:T(512)} %param.28) | copy-start | bytes 6148
  250.8 62.3 %copy-start.5 = (f32[1024]{0:T(1024)S(1)}, f32[1024]{0:T(1024)}, u32[]{:S(2)}) copy-start(f32[1024]{0:T(1024)} %param.30) | copy-start | bytes 12292
  262.8 113.9 %all-reduce.6.cloned.1.call-start = ((), (), s32[]{:S(2)}) async-start(), calls=%async_computation.16 | async-start | bytes 2883584 | tf_op jit(solution)/shard_map/psum | solution.py:42
  313.1 4.1 copy-start.8
  319.1 93.7 %reduce-scatter.26.cloned.1.call-start = ((), (), s32[]{:S(2)}) async-start(), calls=%async_computation.15 | async-start | bytes 589824
Sparse Core Ops, SparseCore 0:
  27.6 58.5 all-reduce.7
  90.8 31.3 reduce-scatter.21
  146.2 22.8 reduce-scatter.17
  171.7 24.1 reduce-scatter.15
  198.5 24.3 reduce-scatter.19
  225.5 24.3 reduce-scatter.13
  262.9 31.2 reduce-scatter.23
  319.2 57.4 all-reduce.5
  381.3 31.4 reduce-scatter.25
